TPU v7x, 32 devices: a whole 2x2x4 slice. The times are simulated.
32 devices in a mesh: grp: 2 (over y), sp: 4 (over z), tp: 4 (over x, core).
Axes of the slice: x: 2, y: 2, z: 4, core: 2. Of those that a mesh axis runs over, the one named last changes fastest.
Arguments:
- tokens: bfloat16 [8, 1024, 2048], P('grp', 'sp'), parts along dimension 0, may hold values from -6 to 6
- norm_gain: bfloat16 [2048], replicated, may hold values from 0.099609375 to 1.8984375
- key_weight: bfloat16 [2048, 2048], P(None, 'tp'), may hold values from -0.125 to 0.125
- value_weight: bfloat16 [2048, 2048], P(None, 'tp'), may hold values from -0.125 to 0.125
- break_bias: bfloat16 [8, 1024, 16], P('grp', 'sp', 'tp'), parts along dimension 0, may hold values from -12 to 0
- new_query: bfloat16 [8, 2048], P('grp', 'tp'), parts along dimension 0, may hold values from -6 to 6
Outputs:
- cache_pair: bfloat16 [8, 4, 256, 2, 2048], P(('grp', 'sp'), None, None, None, 'tp'), parts along dimension 0
- cache_bias: bfloat16 [8, 4, 256, 16], P(('grp', 'sp'), None, None, 'tp'), parts along dimension 0
- attended: float32 [8, 2048], P('grp', 'tp'), parts along dimension 0
There are 2 independent parts, one for each index of `grp`. A program takes and returns all parts, laid end to end along the dimension named above; an argument that names none is the same for every part. Nothing has to cross between parts.
All inputs are finite; a program needn't handle non-finite values.
Results may differ from a plain program's by a relative error of at most 0.0064.
Values may be sent and summed in bfloat16 or wider, within the bound.
No kernel may reach another device: no remote copies, remote signals or barrier semaphores. Data moves between devices by JAX's collectives and lax.ppermute only.
A program may use at most 64 MiB of HBM per device.

v0:
```python
import jax
import jax.numpy as jnp
from jax import lax
from jax.sharding import PartitionSpec as P

norm_eps = 1e-06


def normalize(tokens, norm_gain):
    widened = tokens.astype(jnp.float32)
    inverse = lax.rsqrt(jnp.mean(widened * widened, axis=-1, keepdims=True) + norm_eps)
    return (widened * inverse * norm_gain.astype(jnp.float32)).astype(jnp.bfloat16)


def project(flat_rows, key_weight, value_weight):
    key_rows = jnp.dot(flat_rows, key_weight, preferred_element_type=jnp.float32).astype(
        jnp.bfloat16
    )
    value_rows = jnp.dot(flat_rows, value_weight, preferred_element_type=jnp.float32).astype(
        jnp.bfloat16
    )
    return (key_rows, value_rows)


def read_placed(new_query, key_rows, value_rows, bias_rows, seq_count):
    block_count, piece, heads_here = bias_rows.shape
    columns = key_rows.shape[2]
    head_size = columns // heads_here
    span = block_count // seq_count
    own_index = lax.axis_index("sp")
    own_seq = own_index // span
    own_part = own_index % span
    own_query = lax.dynamic_slice_in_dim(new_query, own_seq, 1, 0).reshape(heads_here, head_size)
    key_heads = key_rows.reshape(block_count, piece, heads_here, head_size)
    logits = jnp.einsum("hd,nphd->nph", own_query, key_heads, preferred_element_type=jnp.float32)
    logits = logits * head_size ** (-0.5) + bias_rows.astype(jnp.float32)
    keep_log = jax.nn.log_sigmoid(-logits)
    block_totals = jnp.sum(keep_log, axis=1)
    own_slot = (jnp.arange(block_count, dtype=jnp.int32) == own_index)[:, None, None]
    placed = jnp.where(own_slot, block_totals[None], 0.0)
    gathered = lax.psum(placed, "sp")
    same_prompt = lax.dynamic_slice_in_dim(gathered, own_seq * span, span, 0)
    ordered = jnp.transpose(same_prompt, (1, 0, 2)).reshape(block_count * span, heads_here)
    beyond = lax.cumsum(ordered, axis=0, reverse=True) - ordered
    beyond = beyond.reshape(block_count, span, heads_here)
    carried = lax.dynamic_slice_in_dim(beyond, own_part, 1, 1)[:, 0, :]
    later_sum = lax.cumsum(keep_log, axis=1, reverse=True) - keep_log + carried[:, None, :]
    stick_weights = jnp.exp(jax.nn.log_sigmoid(logits) + later_sum).astype(jnp.bfloat16)
    value_heads = value_rows.reshape(block_count, piece, heads_here, head_size)
    mixed = jnp.einsum(
        "nph,nphd->hd", stick_weights, value_heads, preferred_element_type=jnp.float32
    )
    chosen = (jnp.arange(seq_count, dtype=jnp.int32) == own_seq)[:, None]
    partial_rows = jnp.where(chosen, mixed.reshape(1, columns), 0.0)
    return lax.psum(partial_rows, "sp")


def local(tokens, norm_gain, key_weight, value_weight, break_bias, new_query):
    seq_count, tok_rows, width = tokens.shape
    heads_here = break_bias.shape[2]
    block_count = lax.axis_size("sp")
    piece = tok_rows * seq_count // block_count
    columns = key_weight.shape[1]
    normed = normalize(tokens, norm_gain)
    bias_pieces = break_bias.reshape(block_count, piece, heads_here)
    key_rows, value_rows = project(normed.reshape(-1, width), key_weight, value_weight)
    stacked_rows = jnp.stack((key_rows, value_rows), axis=1).reshape(block_count, piece, 2, columns)
    paired, bias_arrived = (
        lax.all_to_all(stacked_rows, "sp", split_axis=0, concat_axis=0, tiled=True),
        lax.all_to_all(bias_pieces, "sp", split_axis=0, concat_axis=0, tiled=True),
    )
    key_rows = paired[:, :, 0]
    value_rows = paired[:, :, 1]
    attended = read_placed(new_query, key_rows, value_rows, bias_arrived, seq_count)
    return (paired[None], bias_arrived[None], attended)


def solution(mesh):
    return jax.shard_map(
        local,
        mesh=mesh,
        in_specs=(
            P("grp", "sp", None),
            P(),
            P(None, "tp"),
            P(None, "tp"),
            P("grp", "sp", "tp"),
            P("grp", "tp"),
        ),
        out_specs=(
            P(("grp", "sp"), None, None, None, "tp"),
            P(("grp", "sp"), None, None, "tp"),
            P("grp", "tp"),
        ),
        check_vma=False,
    )
```

profile of v0, /device:TPU:0, one launch (start us, length us, event | category | flops | bytes accessed | tf_op | source)
XLA Modules:
  0.0 130.2 jit_solution(2703418311215314435)
XLA Ops:
  0.6 0.0 copy-start
  0.6 0.0 copy-start.3
  0.7 6.5 %all-to-all-start.1 = ((bf16[4,256,4]{1,2,0:T(4,128)(2,1)}), bf16[4,256,4]{1,2,0:T(4,128)(2,1)S(1)}, u32[]{:S(2)}, u32[]{:S(2)}) async-start(bf16[4,256,4]{1,2,0:T(4,128)(2,1)} %param.10), calls=%async_computation.1 | async-start | bytes 16384 | tf_op jit(solution)/shard_map/all_to_all | solution.py:70
  7.1 0.0 copy-start.1
  7.1 3.2 %fusion = f32[4,256]{1,0:T(4,128)S(1)} fusion(bf16[4,256,2048]{2,1,0:T(8,128)(2,1)} %param.6), kind=kLoop, calls=%fused_computation.2 | loop fusion | flops 6290432 | bytes 4198400 | tf_op jit(solution)/shard_map/reduce_sum | solution.py:11
  10.4 0.0 copy-done.3
  10.4 0.2 copy-done.1
  10.6 1.0 fusion.2
  11.6 0.0 copy-start.2
  11.6 0.0 copy-done
  11.6 3.3 %convolution_convert_fusion.1 = bf16[1024,512]{1,0:T(8,128)(2,1)} fusion(bf16[1024,2048]{1,0:T(8,128)(2,1)S(1)} %bitcast.69, bf16[2048,512]{1,0:T(8,128)(2,1)S(1)} %copy-done), kind=kOutput, calls=%fused_computation.7 | convolution fusion | flops 2148007936 | bytes 7340032 | tf_op jit(solution)/shard_map/dot_general | solution.py:16
  15.0 0.0 copy-done.2
  15.0 1.5 %copy.18 = bf16[4,256,1,512]{1,3,2,0:T(8,128)(2,1)S(1)} copy(bf16[4,256,1,512]{3,1,0,2:T(8,128)(2,1)} %bitcast.72) | data formatting | bytes 2097152 | tf_op jit(solution)/shard_map/stack | solution.py:67
  16.4 6.2 %convolution_convert_fusion = bf16[1024,512]{1,0:T(8,128)(2,1)} fusion(bf16[1024,2048]{1,0:T(8,128)(2,1)} %bitcast.70, bf16[2048,512]{1,0:T(8,128)(2,1)} %param.9), kind=kOutput, calls=%fused_computation.6 | convolution fusion | flops 2148007936 | bytes 7340032 | tf_op jit(solution)/shard_map/dot_general | solution.py:19
  22.6 2.3 %copy.19 = bf16[4,256,1,512]{1,3,2,0:T(8,128)(2,1)} copy(bf16[4,256,1,512]{3,1,0,2:T(8,128)(2,1)} %bitcast.71) | data formatting | bytes 2097152 | tf_op jit(solution)/shard_map/stack | solution.py:67
  24.9 2.7 %pad_maximum_fusion = bf16[4,256,2,512]{1,3,2,0:T(8,128)(2,1)} fusion(bf16[4,256,1,512]{1,3,2,0:T(8,128)(2,1)} %copy.19, bf16[4,256,1,512]{1,3,2,0:T(8,128)(2,1)S(1)} %copy.18), kind=kLoop, calls=%fused_computation.5 | loop fusion | flops 1048576 | bytes 4194304 | tf_op jit(solution)/shard_map/stack | solution.py:67
  27.6 0.0 copy-start.4
  27.6 0.0 all-to-all-done.1
  27.6 5.2 %all-to-all-start = ((bf16[4,256,2,512]{1,3,2,0:T(8,128)(2,1)}), bf16[4,256,2,512]{1,3,2,0:T(8,128)(2,1)}, u32[]{:S(2)}, u32[]{:S(2)}) async-start(bf16[4,256,2,512]{1,3,2,0:T(8,128)(2,1)} %pad_maximum_fusion), calls=%async_computation | async-start | bytes 4194304 | tf_op jit(solution)/shard_map/all_to_all | solution.py:69
  32.8 47.8 %all-to-all-done = bf16[4,256,2,512]{1,3,2,0:T(8,128)(2,1)} async-done(((bf16[4,256,2,512]{1,3,2,0:T(8,128)(2,1)}), bf16[4,256,2,512]{1,3,2,0:T(8,128)(2,1)}, u32[]{:S(2)}, u32[]{:S(2)}) %all-to-all-start) | async-done | bytes 2097184 | tf_op jit(solution)/shard_map/all_to_all | solution.py:69
  80.6 1.7 %fusion.20 = (bf16[4,256,1,512]{1,3,2,0:T(8,128)(2,1)S(1)}, bf16[4,256,1,512]{1,3,2,0:T(8,128)(2,1)S(1)}) fusion(bf16[4,256,2,512]{1,3,2,0:T(8,128)(2,1)} %all-to-all-done), kind=kLoop, calls=%fused_computation.37 | loop fusion | bytes 4194304 | tf_op jit(solution)/shard_map/slice | solution.py:72
  82.3 0.0 copy-done.4
  82.3 0.2 fusion.5
  82.5 0.1 negate_bitcast_fusion
  82.7 0.1 broadcast_select_fusion.1
  82.7 10.0 %psum.14 = f32[4,4,4]{2,1,0:T(4,128)S(1)} all-reduce(f32[4,4,4]{2,1,0:T(4,128)S(1)} %broadcast_select_fusion.1), channel_id=1, replica_groups=mesh['grp'=2,'sp'=4,'tp'=4] {'sp'}, use_global_device_ids=true, to_apply=%region_4.5 | all-reduce | flops 64 | bytes 512 | tf_op jit(solution)/shard_map/psum | solution.py:41
  92.8 20.1 %reduce-window.6 = f32[4,4,2,128]{3,2,1,0:T(2,128)S(1)} reduce-window(f32[4,4,2,128]{3,2,1,0:T(2,128)S(1)} %reshape.54, f32[]{:T(128)} %constant.36.clone.1), window={size=1x1x1x128 pad=0_0x0_0x0_0x0_127}, to_apply=%region_1.2 | reduce-window | flops 520192 | bytes 32772 | tf_op jit(solution)/shard_map/reduce-window
  112.9 0.1 copy.21
  113.1 0.1 copy.22
  113.2 0.1 broadcast_add_fusion
  113.3 0.1 fusion.13
  113.4 0.4 fusion.3
  113.8 0.1 broadcast_select_fusion
  113.8 9.6 %psum.15 = f32[4,512]{1,0:T(4,128)} all-reduce(f32[4,512]{1,0:T(4,128)S(1)} %broadcast_select_fusion), channel_id=1, replica_groups=mesh['grp'=2,'sp'=4,'tp'=4] {'sp'}, use_global_device_ids=true, to_apply=%region_6.7 | all-reduce | flops 2048 | bytes 16384 | tf_op jit(solution)/shard_map/psum | solution.py:55
  123.5 6.2 %copy.24 = bf16[1,4,256,2,512]{4,3,2,1,0:T(2,128)(2,1)} copy(bf16[1,4,256,2,512]{2,4,3,1,0:T(8,128)(2,1)} %bitcast.3) | data formatting | bytes 4194304
  129.6 0.6 copy.51
  (11 shorter events, 0.1 us)
Async XLA Ops:
  0.6 11.0 %copy-start = (bf16[2048,512]{1,0:T(8,128)(2,1)S(1)}, bf16[2048,512]{1,0:T(8,128)(2,1)}, u32[]{:S(2)}) copy-start(bf16[2048,512]{1,0:T(8,128)(2,1)} %param.8) | copy-start | bytes 6291460
  0.6 9.7 %copy-start.3 = (bf16[2048]{0:T(1024)(128)(2,1)S(1)}, bf16[2048]{0:T(1024)(128)(2,1)}, u32[]{:S(2)}) copy-start(bf16[2048]{0:T(1024)(128)(2,1)} %param.7) | copy-start | bytes 12292
  0.7 27.0 %all-to-all-start.1 = ((bf16[4,256,4]{1,2,0:T(4,128)(2,1)}), bf16[4,256,4]{1,2,0:T(4,128)(2,1)S(1)}, u32[]{:S(2)}, u32[]{:S(2)}) async-start(bf16[4,256,4]{1,2,0:T(4,128)(2,1)} %param.10), calls=%async_computation.1 | async-start | bytes 16384 | tf_op jit(solution)/shard_map/all_to_all | solution.py:70
  7.1 3.4 %copy-start.1 = (bf16[4,256,2048]{2,1,0:T(8,128)(2,1)S(1)}, bf16[4,256,2048]{2,1,0:T(8,128)(2,1)}, u32[]{:S(2)}) copy-start(bf16[4,256,2048]{2,1,0:T(8,128)(2,1)} %param.6) | copy-start | bytes 12582916
  11.6 3.3 %copy-start.2 = (bf16[4,256,2048]{2,1,0:T(8,128)(2,1)}, bf16[4,256,2048]{2,1,0:T(8,128)(2,1)S(1)}, u32[]{:S(2)}) copy-start(bf16[4,256,2048]{2,1,0:T(8,128)(2,1)S(1)} %fusion.2) | copy-start | bytes 12582916
  27.6 54.7 %copy-start.4 = (bf16[4,512]{1,0:T(4,128)(2,1)S(1)}, bf16[4,512]{1,0:T(4,128)(2,1)}, u32[]{:S(2)}) copy-start(bf16[4,512]{1,0:T(4,128)(2,1)} %param.11) | copy-start | bytes 12292
  27.6 53.0 %all-to-all-start = ((bf16[4,256,2,512]{1,3,2,0:T(8,128)(2,1)}), bf16[4,256,2,512]{1,3,2,0:T(8,128)(2,1)}, u32[]{:S(2)}, u32[]{:S(2)}) async-start(bf16[4,256,2,512]{1,3,2,0:T(8,128)(2,1)} %pad_maximum_fusion), calls=%async_computation | async-start | bytes 4194304 | tf_op jit(solution)/shard_map/all_to_all | solution.py:69
where the time goes:
time: 131 us; the launch traced here: 130 us
  waiting for transfers between devices  47.8 us (36%)
  other arithmetic  27.6 us (21%)
  blocking collectives  19.6 us (15%)
  local copies, waits for them, and re-layouts  12.7 us (10%)
  starting transfers between devices  11.7 us (9%)
  matrix products  10.1 us (8%)
    all_to_all x1, waiting for transfers between devices, local(): lax.all_to_all(stacked_rows, 'sp', split_axis=0, concat_axis=0, tiled=True)  47.8 us
    another operation x2, other arithmetic  20.1 us
    psum x1, blocking collectives, read_placed(): gathered = lax.psum(placed, 'sp')  9.95 us
    psum x1, blocking collectives, read_placed(): return lax.psum(partial_rows, 'sp')  9.64 us
    unnamed x12, local copies, waits for them, and re-layouts  6.96 us
    all_to_all x1, starting transfers between devices, local(): lax.all_to_all(bias_pieces, 'sp', split_axis=0, concat_axis=0, tiled=True)  6.49 us
    dot_general x1, matrix products, project(): jnp.dot(flat_rows, value_weight, preferred_element_type=jnp.float32)  6.16 us
    all_to_all x1, starting transfers between devices, local(): lax.all_to_all(stacked_rows, 'sp', split_axis=0, concat_axis=0, tiled=True)  5.22 us
  transfers between devices with their start and end apart: 2, of which 1 were waited for; matrix products, arithmetic and copies ran while one was open for 16% of the time, Pallas kernels for 0%

commit v1 on v0

--- a/solution.py
+++ b/solution.py
@@ -38,7 +38,7 @@
     block_totals = jnp.sum(keep_log, axis=1)
     own_slot = (jnp.arange(block_count, dtype=jnp.int32) == own_index)[:, None, None]
     placed = jnp.where(own_slot, block_totals[None], 0.0)
-    gathered = lax.psum(placed, "sp")
+    gathered = jnp.sum(lax.all_gather(placed, "sp"), axis=0)
     same_prompt = lax.dynamic_slice_in_dim(gathered, own_seq * span, span, 0)
     ordered = jnp.transpose(same_prompt, (1, 0, 2)).reshape(block_count * span, heads_here)
     beyond = lax.cumsum(ordered, axis=0, reverse=True) - ordered

time: 131 us -> 135 us (1.031)
  blocking collectives: 19.6 us -> 23.7 us
    all_gather x0 -> x1, blocking collectives: none -> 13.1 us  [read_placed(): gathered = jnp.sum(lax.all_gather(placed, 'sp'), axis=0)]
    psum x1 -> x0, blocking collectives: 9.95 us -> none  [read_placed(): gathered = lax.psum(placed, 'sp')]
  transfers between devices with their start and end apart: 2 -> 2, of which waited for: 1 -> 1; matrix products, arithmetic and copies ran while one was open for 16% -> 15% of each run, Pallas kernels for 0% -> 0%
where the time goes in v1:
time: 135 us; the launch traced here: 134 us
  waiting for transfers between devices  47.8 us (35%)
  other arithmetic  27.6 us (20%)
  blocking collectives  23.7 us (18%)
  local copies, waits for them, and re-layouts  12.7 us (9%)
  starting transfers between devices  11.7 us (9%)
  matrix products  10.1 us (7%)
    all_to_all x1, waiting for transfers between devices, local(): lax.all_to_all(stacked_rows, 'sp', split_axis=0, concat_axis=0, tiled=True)  47.8 us
    another operation x2, other arithmetic  20.1 us
    all_gather x1, blocking collectives, read_placed(): gathered = jnp.sum(lax.all_gather(placed, 'sp'), axis=0)  13.1 us
    psum x1, blocking collectives, read_placed(): return lax.psum(partial_rows, 'sp')  10.6 us
    unnamed x12, local copies, waits for them, and re-layouts  6.96 us
    all_to_all x1, starting transfers between devices, local(): lax.all_to_all(bias_pieces, 'sp', split_axis=0, concat_axis=0, tiled=True)  6.49 us
    dot_general x1, matrix products, project(): jnp.dot(flat_rows, value_weight, preferred_element_type=jnp.float32)  6.16 us
    all_to_all x1, starting transfers between devices, local(): lax.all_to_all(stacked_rows, 'sp', split_axis=0, concat_axis=0, tiled=True)  5.22 us
  transfers between devices with their start and end apart: 2, of which 1 were waited for; matrix products, arithmetic and copies ran while one was open for 15% of the time, Pallas kernels for 0%

profile of v1, /device:TPU:0, one launch (start us, length us, event | category | flops | bytes accessed | tf_op | source)
XLA Modules:
  0.0 134.3 jit_solution(3318801790928387108)
XLA Ops:
  0.6 0.0 copy-start
  0.6 0.0 copy-start.3
  0.7 6.5 %all-to-all-start.1 = ((bf16[4,256,4]{1,2,0:T(4,128)(2,1)}), bf16[4,256,4]{1,2,0:T(4,128)(2,1)S(1)}, u32[]{:S(2)}, u32[]{:S(2)}) async-start(bf16[4,256,4]{1,2,0:T(4,128)(2,1)} %param.10), calls=%async_computation.1 | async-start | bytes 16384 | tf_op jit(solution)/shard_map/all_to_all | solution.py:70
  7.1 0.0 copy-start.1
  7.1 3.2 %fusion = f32[4,256]{1,0:T(4,128)S(1)} fusion(bf16[4,256,2048]{2,1,0:T(8,128)(2,1)} %param.6), kind=kLoop, calls=%fused_computation.2 | loop fusion | flops 6290432 | bytes 4198400 | tf_op jit(solution)/shard_map/reduce_sum | solution.py:11
  10.4 0.0 copy-done.3
  10.4 0.2 copy-done.1
  10.6 1.0 fusion.2
  11.6 0.0 copy-start.2
  11.6 0.0 copy-done
  11.6 3.3 %convolution_convert_fusion.1 = bf16[1024,512]{1,0:T(8,128)(2,1)} fusion(bf16[1024,2048]{1,0:T(8,128)(2,1)S(1)} %bitcast.69, bf16[2048,512]{1,0:T(8,128)(2,1)S(1)} %copy-done), kind=kOutput, calls=%fused_computation.7 | convolution fusion | flops 2148007936 | bytes 7340032 | tf_op jit(solution)/shard_map/dot_general | solution.py:16
  15.0 0.0 copy-done.2
  15.0 1.5 %copy.18 = bf16[4,256,1,512]{1,3,2,0:T(8,128)(2,1)S(1)} copy(bf16[4,256,1,512]{3,1,0,2:T(8,128)(2,1)} %bitcast.72) | data formatting | bytes 2097152 | tf_op jit(solution)/shard_map/stack | solution.py:67
  16.4 6.2 %convolution_convert_fusion = bf16[1024,512]{1,0:T(8,128)(2,1)} fusion(bf16[1024,2048]{1,0:T(8,128)(2,1)} %bitcast.70, bf16[2048,512]{1,0:T(8,128)(2,1)} %param.9), kind=kOutput, calls=%fused_computation.6 | convolution fusion | flops 2148007936 | bytes 7340032 | tf_op jit(solution)/shard_map/dot_general | solution.py:19
  22.6 2.3 %copy.19 = bf16[4,256,1,512]{1,3,2,0:T(8,128)(2,1)} copy(bf16[4,256,1,512]{3,1,0,2:T(8,128)(2,1)} %bitcast.71) | data formatting | bytes 2097152 | tf_op jit(solution)/shard_map/stack | solution.py:67
  24.9 2.7 %pad_maximum_fusion = bf16[4,256,2,512]{1,3,2,0:T(8,128)(2,1)} fusion(bf16[4,256,1,512]{1,3,2,0:T(8,128)(2,1)} %copy.19, bf16[4,256,1,512]{1,3,2,0:T(8,128)(2,1)S(1)} %copy.18), kind=kLoop, calls=%fused_computation.5 | loop fusion | flops 1048576 | bytes 4194304 | tf_op jit(solution)/shard_map/stack | solution.py:67
  27.6 0.0 copy-start.4
  27.6 0.0 all-to-all-done.1
  27.6 5.2 %all-to-all-start = ((bf16[4,256,2,512]{1,3,2,0:T(8,128)(2,1)}), bf16[4,256,2,512]{1,3,2,0:T(8,128)(2,1)}, u32[]{:S(2)}, u32[]{:S(2)}) async-start(bf16[4,256,2,512]{1,3,2,0:T(8,128)(2,1)} %pad_maximum_fusion), calls=%async_computation | async-start | bytes 4194304 | tf_op jit(solution)/shard_map/all_to_all | solution.py:69
  32.8 47.8 %all-to-all-done = bf16[4,256,2,512]{1,3,2,0:T(8,128)(2,1)} async-done(((bf16[4,256,2,512]{1,3,2,0:T(8,128)(2,1)}), bf16[4,256,2,512]{1,3,2,0:T(8,128)(2,1)}, u32[]{:S(2)}, u32[]{:S(2)}) %all-to-all-start) | async-done | bytes 2097184 | tf_op jit(solution)/shard_map/all_to_all | solution.py:69
  80.6 1.7 %fusion.20 = (bf16[4,256,1,512]{1,3,2,0:T(8,128)(2,1)S(1)}, bf16[4,256,1,512]{1,3,2,0:T(8,128)(2,1)S(1)}) fusion(bf16[4,256,2,512]{1,3,2,0:T(8,128)(2,1)} %all-to-all-done), kind=kLoop, calls=%fused_computation.37 | loop fusion | bytes 4194304 | tf_op jit(solution)/shard_map/slice | solution.py:72
  82.3 0.0 copy-done.4
  82.3 0.2 fusion.5
  82.5 0.1 negate_bitcast_fusion
  82.7 0.1 broadcast_select_fusion.1
  82.7 13.1 %all_gather.4 = f32[4,4,4,4]{3,2,1,0:T(4,128)S(1)} all-gather(f32[1,4,4,4]{3,2,1,0:T(4,128)S(1)} %broadcast_select_fusion.1), channel_id=1, replica_groups=mesh['grp'=2,'sp'=4,'tp'=4] {'sp'}, dimensions={0}, use_global_device_ids=true | all-gather | bytes 1280 | tf_op jit(solution)/shard_map/all_gather | solution.py:41
  96.0 20.1 %reduce-window.6 = f32[4,4,2,128]{3,2,1,0:T(2,128)S(1)} reduce-window(f32[4,4,2,128]{3,2,1,0:T(2,128)S(1)} %reshape.57, f32[]{:T(128)} %constant.36.clone.1), window={size=1x1x1x128 pad=0_0x0_0x0_0x0_127}, to_apply=%region_1.2 | reduce-window | flops 520192 | bytes 32772 | tf_op jit(solution)/shard_map/reduce-window
  116.1 0.1 copy.21
  116.3 0.1 copy.22
  116.4 0.1 broadcast_add_fusion
  116.5 0.1 fusion.13
  116.6 0.4 fusion.3
  117.0 0.1 broadcast_select_fusion
  117.0 10.6 %psum.7 = f32[4,512]{1,0:T(4,128)} all-reduce(f32[4,512]{1,0:T(4,128)S(1)} %broadcast_select_fusion), channel_id=1, replica_groups=mesh['grp'=2,'sp'=4,'tp'=4] {'sp'}, use_global_device_ids=true, to_apply=%region_6.7 | all-reduce | flops 2048 | bytes 16384 | tf_op jit(solution)/shard_map/psum | solution.py:55
  127.6 6.2 %copy.24 = bf16[1,4,256,2,512]{4,3,2,1,0:T(2,128)(2,1)} copy(bf16[1,4,256,2,512]{2,4,3,1,0:T(8,128)(2,1)} %bitcast.3) | data formatting | bytes 4194304
  133.7 0.6 copy.51
  (12 shorter events, 0.2 us)
Async XLA Ops:
  0.6 11.0 %copy-start = (bf16[2048,512]{1,0:T(8,128)(2,1)S(1)}, bf16[2048,512]{1,0:T(8,128)(2,1)}, u32[]{:S(2)}) copy-start(bf16[2048,512]{1,0:T(8,128)(2,1)} %param.8) | copy-start | bytes 6291460
  0.6 9.7 %copy-start.3 = (bf16[2048]{0:T(1024)(128)(2,1)S(1)}, bf16[2048]{0:T(1024)(128)(2,1)}, u32[]{:S(2)}) copy-start(bf16[2048]{0:T(1024)(128)(2,1)} %param.7) | copy-start | bytes 12292
  0.7 27.0 %all-to-all-start.1 = ((bf16[4,256,4]{1,2,0:T(4,128)(2,1)}), bf16[4,256,4]{1,2,0:T(4,128)(2,1)S(1)}, u32[]{:S(2)}, u32[]{:S(2)}) async-start(bf16[4,256,4]{1,2,0:T(4,128)(2,1)} %param.10), calls=%async_computation.1 | async-start | bytes 16384 | tf_op jit(solution)/shard_map/all_to_all | solution.py:70
  7.1 3.4 %copy-start.1 = (bf16[4,256,2048]{2,1,0:T(8,128)(2,1)S(1)}, bf16[4,256,2048]{2,1,0:T(8,128)(2,1)}, u32[]{:S(2)}) copy-start(bf16[4,256,2048]{2,1,0:T(8,128)(2,1)} %param.6) | copy-start | bytes 12582916
  11.6 3.3 %copy-start.2 = (bf16[4,256,2048]{2,1,0:T(8,128)(2,1)}, bf16[4,256,2048]{2,1,0:T(8,128)(2,1)S(1)}, u32[]{:S(2)}) copy-start(bf16[4,256,2048]{2,1,0:T(8,128)(2,1)S(1)} %fusion.2) | copy-start | bytes 12582916
  27.6 54.7 %copy-start.4 = (bf16[4,512]{1,0:T(4,128)(2,1)S(1)}, bf16[4,512]{1,0:T(4,128)(2,1)}, u32[]{:S(2)}) copy-start(bf16[4,512]{1,0:T(4,128)(2,1)} %param.11) | copy-start | bytes 12292
  27.6 53.0 %all-to-all-start = ((bf16[4,256,2,512]{1,3,2,0:T(8,128)(2,1)}), bf16[4,256,2,512]{1,3,2,0:T(8,128)(2,1)}, u32[]{:S(2)}, u32[]{:S(2)}) async-start(bf16[4,256,2,512]{1,3,2,0:T(8,128)(2,1)} %pad_maximum_fusion), calls=%async_computation | async-start | bytes 4194304 | tf_op jit(solution)/shard_map/all_to_all | solution.py:69
